TPU v7x, 32 devices: a whole 2x2x4 slice. The times are simulated.
32 devices in a mesh: ep: 8 (over z, core), tp: 4 (over y, x).
Axes of the slice: x: 2, y: 2, z: 4, core: 2. Of those that a mesh axis runs over, the one named last changes fastest.
Arguments:
- tokens: bfloat16 [1024, 4096], P('ep', 'tp'), may hold values from -6 to 6
- routes: int32 [1024, 2], P('ep'), may hold values from 0 to 15, all different within a row; in each aligned block of 128 rows (0 to 127, 128 to 255, ...) at most 20 rows name the same one
- route_weights: float32 [1024, 2], P('ep'), may hold values from 0.2 to 2
- cotangent: bfloat16 [1024, 4096], P('ep', 'tp'), may hold values from -6 to 6
- expert_gate: bfloat16 [16, 4096, 512], P('ep', 'tp'), may hold values from -0.09375 to 0.09375
- expert_up: bfloat16 [16, 4096, 512], P('ep', 'tp'), may hold values from -0.09375 to 0.09375
- expert_down: bfloat16 [16, 512, 4096], P('ep', None, 'tp'), may hold values from -0.25 to 0.25
- shared_gate: bfloat16 [4096, 512], P('tp'), may hold values from -0.09375 to 0.09375
- shared_up: bfloat16 [4096, 512], P('tp'), may hold values from -0.09375 to 0.09375
- shared_down: bfloat16 [512, 4096], P(None, 'tp'), may hold values from -0.25 to 0.25
Outputs:
- grad_tokens: bfloat16 [1024, 4096], P('ep', 'tp')
- grad_weights: float32 [1024, 2], P('ep')
- grad_expert_gate: float32 [16, 4096, 512], P('ep', 'tp')
- grad_expert_up: float32 [16, 4096, 512], P('ep', 'tp')
- grad_expert_down: float32 [16, 512, 4096], P('ep', None, 'tp')
- grad_shared_gate: float32 [4096, 512], P('tp', 'ep')
- grad_shared_up: float32 [4096, 512], P('tp', 'ep')
- grad_shared_down: float32 [512, 4096], P('ep', 'tp')
Inputs may be any that keep to these rules, and one draw needn't show every extreme that they name: `routes`: each row names 2 different experts. In each aligned block of 128 rows (the rows of one index of ep) no expert is named by more than 20 rows, a bound that some block reaches.
All inputs are finite; a program needn't handle non-finite values.
Results may differ from a plain program's by a relative error of at most 0.0054.
Values may be sent and summed in bfloat16 or wider, within the bound.
A program may use at most 64 MiB of HBM per device.

v0:
```python
import jax
import jax.numpy as jnp
from jax import lax
from jax.sharding import PartitionSpec as P


def hidden_terms(gate_pre, up_pre, back_grad, scaling):
    logistic = jax.nn.sigmoid(gate_pre)
    product = gate_pre * logistic * up_pre
    grad_act = scaling * back_grad
    gate_grad = (grad_act * up_pre * logistic * (1.0 + gate_pre * (1.0 - logistic))).astype(
        jnp.bfloat16
    )
    up_grad = (grad_act * gate_pre * logistic).astype(jnp.bfloat16)
    hidden = (scaling * product).astype(jnp.bfloat16)
    return (gate_grad, up_grad, hidden, jnp.sum(back_grad * product, axis=-1))


def shared_weight_sums(tokens, cotangent, shared_gate_grad, shared_up_grad, shared_hidden):
    local_gate = jnp.einsum(
        "td,tf->df", tokens, shared_gate_grad, preferred_element_type=jnp.float32
    )
    local_up = jnp.einsum("td,tf->df", tokens, shared_up_grad, preferred_element_type=jnp.float32)
    local_down = jnp.einsum(
        "tf,td->fd", shared_hidden, cotangent, preferred_element_type=jnp.float32
    )
    return (
        lax.psum_scatter(local_gate, "ep", scatter_dimension=1, tiled=True),
        lax.psum_scatter(local_up, "ep", scatter_dimension=1, tiled=True),
        lax.psum_scatter(local_down, "ep", scatter_dimension=0, tiled=True),
    )


def body(
    tokens,
    routes,
    route_weights,
    cotangent,
    expert_gate,
    expert_up,
    expert_down,
    shared_gate,
    shared_up,
    shared_down,
):
    tok_rows, top_count = routes.shape
    feat_cols = tokens.shape[1]
    local_experts = expert_gate.shape[0]
    group_size = lax.axis_size("ep")
    capacity = max(2, 5 * tok_rows * top_count // (4 * group_size * local_experts))
    all_experts = group_size * local_experts
    picked = routes.reshape(-1)
    onehot = (picked[:, None] == jnp.arange(all_experts, dtype=jnp.int32)[None, :]).astype(
        jnp.int32
    )
    ranked = jnp.sum(jnp.cumsum(onehot, axis=0) * onehot, axis=1) - 1
    slot_ids = picked * capacity + ranked
    places = (
        jnp.arange(all_experts * capacity, dtype=jnp.int32)[:, None] == slot_ids[None, :]
    ).astype(jnp.bfloat16)
    repeat_tokens = jnp.repeat(tokens, top_count, axis=0)
    repeat_cotan = jnp.repeat(cotangent, top_count, axis=0)
    gate_bf = route_weights.reshape(-1).astype(jnp.bfloat16)
    send_tokens = jnp.dot(places, repeat_tokens, preferred_element_type=jnp.float32).astype(
        jnp.bfloat16
    )
    send_cotan = jnp.dot(places, repeat_cotan, preferred_element_type=jnp.float32).astype(
        jnp.bfloat16
    )
    send_gates = jnp.dot(places, gate_bf, preferred_element_type=jnp.float32).astype(jnp.bfloat16)
    send_tokens = send_tokens.reshape(group_size, local_experts, capacity, feat_cols)
    send_cotan = send_cotan.reshape(group_size, local_experts, capacity, feat_cols)
    send_gates = send_gates.reshape(group_size, local_experts, capacity)
    got_tokens, got_cotan, got_gates = (
        lax.all_to_all(send_tokens, "ep", split_axis=0, concat_axis=2, tiled=True),
        lax.all_to_all(send_cotan, "ep", split_axis=0, concat_axis=2, tiled=True),
        lax.all_to_all(send_gates, "ep", split_axis=0, concat_axis=2, tiled=True),
    )
    slot_tokens = got_tokens[0]
    slot_cotan = got_cotan[0]
    slot_gates = got_gates[0].astype(jnp.float32)
    part_gate = jnp.einsum(
        "esd,edf->esf", slot_tokens, expert_gate, preferred_element_type=jnp.float32
    )
    part_up = jnp.einsum("esd,edf->esf", slot_tokens, expert_up, preferred_element_type=jnp.float32)
    part_down = jnp.einsum(
        "esd,efd->esf", slot_cotan, expert_down, preferred_element_type=jnp.float32
    )
    gate_pre, up_pre, back_grad = lax.psum((part_gate, part_up, part_down), "tp")
    gate_grad, up_grad, hidden, slot_dg = hidden_terms(
        gate_pre, up_pre, back_grad, slot_gates[:, :, None]
    )
    shared_part_gate = jnp.dot(tokens, shared_gate, preferred_element_type=jnp.float32)
    shared_part_up = jnp.dot(tokens, shared_up, preferred_element_type=jnp.float32)
    shared_part_down = jnp.einsum(
        "td,fd->tf", cotangent, shared_down, preferred_element_type=jnp.float32
    )
    share_gate_pre, share_up_pre, share_back = (
        lax.psum_scatter(shared_part_gate, "tp", scatter_dimension=1, tiled=True),
        lax.psum_scatter(shared_part_up, "tp", scatter_dimension=1, tiled=True),
        lax.psum_scatter(shared_part_down, "tp", scatter_dimension=1, tiled=True),
    )
    share_gate_grad, share_up_grad, share_hidden, unused_sum = hidden_terms(
        share_gate_pre, share_up_pre, share_back, 1.0
    )
    shared_gate_grad, shared_up_grad, shared_hidden = (
        lax.all_gather(share_gate_grad, "tp", axis=1, tiled=True),
        lax.all_gather(share_up_grad, "tp", axis=1, tiled=True),
        lax.all_gather(share_hidden, "tp", axis=1, tiled=True),
    )
    slot_grad = jnp.einsum(
        "esf,edf->esd", gate_grad, expert_gate, preferred_element_type=jnp.float32
    ) + jnp.einsum("esf,edf->esd", up_grad, expert_up, preferred_element_type=jnp.float32)
    grad_expert_gate = jnp.einsum(
        "esd,esf->edf", slot_tokens, gate_grad, preferred_element_type=jnp.float32
    )
    grad_expert_up = jnp.einsum(
        "esd,esf->edf", slot_tokens, up_grad, preferred_element_type=jnp.float32
    )
    grad_expert_down = jnp.einsum(
        "esf,esd->efd", hidden, slot_cotan, preferred_element_type=jnp.float32
    )
    back_rows, back_dg = (
        lax.all_to_all(slot_grad, "ep", split_axis=1, concat_axis=0, tiled=True),
        lax.all_to_all(slot_dg, "ep", split_axis=1, concat_axis=0, tiled=True),
    )
    back_rows = back_rows.reshape(all_experts * capacity, feat_cols)
    back_dg = back_dg.reshape(all_experts * capacity)
    routed_grad = jnp.sum(
        jnp.take(back_rows, slot_ids, axis=0).reshape(tok_rows, top_count, feat_cols), axis=1
    )
    grad_weights = jnp.take(back_dg, slot_ids).reshape(tok_rows, top_count)
    shared_grad = jnp.einsum(
        "tf,df->td", shared_gate_grad, shared_gate, preferred_element_type=jnp.float32
    ) + jnp.einsum("tf,df->td", shared_up_grad, shared_up, preferred_element_type=jnp.float32)
    grad_shared_gate, grad_shared_up, grad_shared_down = shared_weight_sums(
        tokens, cotangent, shared_gate_grad, shared_up_grad, shared_hidden
    )
    grad_tokens = (routed_grad + shared_grad).astype(jnp.bfloat16)
    return (
        grad_tokens,
        grad_weights,
        grad_expert_gate,
        grad_expert_up,
        grad_expert_down,
        grad_shared_gate,
        grad_shared_up,
        grad_shared_down,
    )


def solution(mesh):
    return jax.shard_map(
        body,
        mesh=mesh,
        in_specs=(
            P("ep", "tp"),
            P("ep", None),
            P("ep", None),
            P("ep", "tp"),
            P("ep", "tp", None),
            P("ep", "tp", None),
            P("ep", None, "tp"),
            P("tp", None),
            P("tp", None),
            P(None, "tp"),
        ),
        out_specs=(
            P("ep", "tp"),
            P("ep", None),
            P("ep", "tp", None),
            P("ep", "tp", None),
            P("ep", None, "tp"),
            P("tp", "ep"),
            P("tp", "ep"),
            P("ep", "tp"),
        ),
        check_vma=False,
    )
```

profile of v0, /device:TPU:0, one launch (start us, length us, event | category | flops | bytes accessed | tf_op | source)
XLA Modules:
  0.0 318.2 jit_solution(8350783639700550073)
XLA Ops:
  12.8 6.4 %all-to-all-start.2 = ((bf16[8,2,20,1024]{3,1,2,0:T(2,128)(2,1)}), bf16[8,2,20,1024]{3,1,2,0:T(2,128)(2,1)S(1)}, u32[]{:S(2)}, u32[]{:S(2)}) async-start(bf16[8,2,20,1024]{3,1,2,0:T(2,128)(2,1)} %copy.64), calls=%async_computation.2 | async-start | bytes 1310720 | tf_op jit(solution)/shard_map/all_to_all | solution.py:75
  29.0 2.6 copy.62
  31.7 5.6 %all-to-all-done.2 = bf16[8,2,20,1024]{3,1,2,0:T(2,128)(2,1)S(1)} async-done(((bf16[8,2,20,1024]{3,1,2,0:T(2,128)(2,1)}), bf16[8,2,20,1024]{3,1,2,0:T(2,128)(2,1)S(1)}, u32[]{:S(2)}, u32[]{:S(2)}) %all-to-all-start.2) | async-done | bytes 655392 | tf_op jit(solution)/shard_map/all_to_all | solution.py:75
  37.3 4.2 %all-to-all-start.1 = ((bf16[8,2,20,1024]{3,1,2,0:T(2,128)(2,1)}), bf16[8,2,20,1024]{3,1,2,0:T(2,128)(2,1)}, u32[]{:S(2)}, u32[]{:S(2)}) async-start(bf16[8,2,20,1024]{3,1,2,0:T(2,128)(2,1)} %copy.62), calls=%async_computation.1 | async-start | bytes 1310720 | tf_op jit(solution)/shard_map/all_to_all | solution.py:76
  49.3 10.3 %all-to-all-done.1 = bf16[8,2,20,1024]{3,1,2,0:T(2,128)(2,1)} async-done(((bf16[8,2,20,1024]{3,1,2,0:T(2,128)(2,1)}), bf16[8,2,20,1024]{3,1,2,0:T(2,128)(2,1)}, u32[]{:S(2)}, u32[]{:S(2)}) %all-to-all-start.1) | async-done | bytes 655392 | tf_op jit(solution)/shard_map/all_to_all | solution.py:76
  59.6 3.5 %fusion.4 = f32[2,160,512]{2,1,0:T(8,128)} fusion(bf16[2,512,1024]{2,1,0:T(8,128)(2,1)} %param.16, bf16[2,160,1024]{2,0,1:T(2,128)(2,1)} %bitcast.5), kind=kOutput, calls=%fused_computation.20 | convolution fusion | flops 335544320 | bytes 3407872 | tf_op jit(solution)/shard_map/esd,efd->esf/dot_general | solution.py:86
  63.2 13.6 %reduce-scatter.11.cloned.1.call-done = f32[128,128]{1,0:T(8,128)} async-done(((f32[128,512]{1,0:T(8,128)}), f32[128,128]{1,0:T(8,128)}) %reduce-scatter.11.cloned.1.call-update) | async-done | bytes 65552 | tf_op jit(solution)/shard_map/reduce_scatter | solution.py:99
  76.8 27.7 %reduce-scatter.9.cloned.1.call-done = f32[128,128]{1,0:T(8,128)} async-done(((f32[128,512]{1,0:T(8,128)}), f32[128,128]{1,0:T(8,128)}) %reduce-scatter.9.cloned.1.call-update) | async-done | bytes 65552 | tf_op jit(solution)/shard_map/reduce_scatter | solution.py:100
  105.5 8.5 %all_gather.10 = bf16[128,512]{1,0:T(8,128)(2,1)S(1)} all-gather(bf16[128,128]{1,0:T(8,128)(2,1)S(1)} %get-tuple-element.42), channel_id=1, replica_groups=mesh['ep'=8,'tp'=4] {'tp'}, dimensions={1}, use_global_device_ids=true | all-gather | bytes 163840 | tf_op jit(solution)/shard_map/all_gather | solution.py:108
  116.5 8.8 %all_gather.9 = bf16[128,512]{1,0:T(8,128)(2,1)S(1)} all-gather(bf16[128,128]{1,0:T(8,128)(2,1)S(1)} %get-tuple-element.41), channel_id=1, replica_groups=mesh['ep'=8,'tp'=4] {'tp'}, dimensions={1}, use_global_device_ids=true | all-gather | bytes 163840 | tf_op jit(solution)/shard_map/all_gather | solution.py:107
  127.8 8.3 %all_gather.11 = bf16[128,512]{1,0:T(8,128)(2,1)S(1)} all-gather(bf16[128,128]{1,0:T(8,128)(2,1)S(1)} %get-tuple-element.40), channel_id=1, replica_groups=mesh['ep'=8,'tp'=4] {'tp'}, dimensions={1}, use_global_device_ids=true | all-gather | bytes 163840 | tf_op jit(solution)/shard_map/all_gather | solution.py:109
  138.6 10.0 %all_to_all.70 = bf16[8,2,20]{2,1,0:T(2,128)(2,1)S(1)} all-to-all(bf16[8,2,20]{2,1,0:T(2,128)(2,1)S(1)} %reshape.139), channel_id=1, replica_groups=mesh['ep'=8,'tp'=4] {'ep'}, dimensions={0} | all-to-all | bytes 1280 | tf_op jit(solution)/shard_map/all_to_all | solution.py:77
  148.6 28.3 %all-reduce.3.cloned.1.call-done = (f32[2,160,512]{2,1,0:T(8,128)}, f32[2,160,512]{2,1,0:T(8,128)}, f32[2,160,512]{2,1,0:T(8,128)}) async-done(((f32[2,160,512]{2,1,0:T(8,128)}, f32[2,160,512]{2,1,0:T(8,128)}, f32[2,160,512]{2,1,0:T(8,128)}), (f32[2,160,512]{2,1,0:T(8,128)}, f32[2,160,512]{2,1,0:T(8,128)}, f32[2,160,512]{2,1,0:T(8,128)})) %all-reduce.3.cloned.1.call-update) | async-done | bytes 1966096 | tf_op jit(solution)/shard_map/psum | solution.py:89
  179.6 4.6 %all-to-all-start.4 = ((f32[2,8,20]{2,0,1:T(2,128)}), f32[2,8,20]{2,0,1:T(2,128)S(1)}, u32[]{:S(2)}, u32[]{:S(2)}) async-start(f32[2,8,20]{2,0,1:T(2,128)} %copy.69), calls=%async_computation.7 | async-start | bytes 16384 | tf_op jit(solution)/shard_map/all_to_all | solution.py:125
  189.8 4.5 %all-to-all-start.3 = ((f32[2,160,1024]{2,0,1:T(2,128)}), f32[2,160,1024]{2,0,1:T(2,128)}, u32[]{:S(2)}, u32[]{:S(2)}) async-start(f32[2,160,1024]{2,0,1:T(2,128)} %copy.67), calls=%async_computation.3 | async-start | bytes 2621440 | tf_op jit(solution)/shard_map/all_to_all | solution.py:124
  199.9 2.8 fusion.6
  202.7 2.8 fusion.8
  205.6 4.0 %fusion.2 = f32[2,512,1024]{2,1,0:T(8,128)} fusion(bf16[2,160,1024]{2,0,1:T(2,128)(2,1)} %bitcast.5, f32[2,160]{1,0:T(2,128)S(1)} %reshape.146, f32[2,160,512]{2,1,0:T(8,128)S(1)} %copy-done.6, f32[2,160,512]{2,1,0:T(8,128)S(1)} %copy-done.5), kind=kOutput, calls=%fused_computation.18 | convolution fusion | flops 336691200 | bytes 6161664 | tf_op jit(solution)/shard_map/esf,esd->efd/dot_general | solution.py:120
  212.5 25.8 %all-to-all-done.3 = f32[2,160,1024]{2,0,1:T(2,128)} async-done(((f32[2,160,1024]{2,0,1:T(2,128)}), f32[2,160,1024]{2,0,1:T(2,128)}, u32[]{:S(2)}, u32[]{:S(2)}) %all-to-all-start.3) | async-done | bytes 1310752 | tf_op jit(solution)/shard_map/all_to_all | solution.py:124
  238.3 2.9 copy.68
  244.8 2.9 gather.13
  247.7 2.7 select_reduce_fusion
  252.7 21.1 %reduce-scatter.13.cloned.1.call-done = f32[1024,64]{0,1:T(8,128)} async-done(((f32[1024,512]{0,1:T(8,128)}), f32[1024,64]{0,1:T(8,128)}) %reduce-scatter.13.cloned.1.call-update) | async-done | bytes 262160 | tf_op jit(solution)/shard_map/reduce_scatter | solution.py:28
  273.8 37.6 %reduce-scatter.17.cloned.1.call-done = f32[64,1024]{1,0:T(8,128)} async-done(((f32[512,1024]{1,0:T(8,128)}), f32[64,1024]{1,0:T(8,128)}) %reduce-scatter.17.cloned.1.call-update) | async-done | bytes 262160 | tf_op jit(solution)/shard_map/reduce_scatter | solution.py:30
  (103 shorter events, 54.3 us)
Async XLA Ops:
  7.2 39.1 %copy-start = (bf16[2,1024,512]{2,1,0:T(8,128)(2,1)S(1)}, bf16[2,1024,512]{2,1,0:T(8,128)(2,1)}, u32[]{:S(2)}) copy-start(bf16[2,1024,512]{2,1,0:T(8,128)(2,1)} %param.14) | copy-start | bytes 6291460
  8.1 1.2 copy-start.8
  11.3 7.9 %copy-start.7 = (bf16[128,1024]{1,0:T(8,128)(2,1)S(1)}, bf16[128,1024]{1,0:T(8,128)(2,1)}, u32[]{:S(2)}) copy-start(bf16[128,1024]{1,0:T(8,128)(2,1)} %param.13) | copy-start | bytes 786436
  12.8 24.5 %all-to-all-start.2 = ((bf16[8,2,20,1024]{3,1,2,0:T(2,128)(2,1)}), bf16[8,2,20,1024]{3,1,2,0:T(2,128)(2,1)S(1)}, u32[]{:S(2)}, u32[]{:S(2)}) async-start(bf16[8,2,20,1024]{3,1,2,0:T(2,128)(2,1)} %copy.64), calls=%async_computation.2 | async-start | bytes 1310720 | tf_op jit(solution)/shard_map/all_to_all | solution.py:75
  19.1 44.1 %reduce-scatter.7.cloned.1.call-start = ((), (), s32[]{:S(2)}) async-start(), calls=%async_computation.11 | async-start | bytes 327680 | tf_op jit(solution)/shard_map/reduce_scatter | solution.py:101
  27.0 14.6 %copy-start.3 = (bf16[128,1024]{1,0:T(8,128)(2,1)S(1)}, bf16[128,1024]{1,0:T(8,128)(2,1)}, u32[]{:S(2)}) copy-start(bf16[128,1024]{1,0:T(8,128)(2,1)} %param.10) | copy-start | bytes 786436
  37.3 22.4 %all-to-all-start.1 = ((bf16[8,2,20,1024]{3,1,2,0:T(2,128)(2,1)}), bf16[8,2,20,1024]{3,1,2,0:T(2,128)(2,1)}, u32[]{:S(2)}, u32[]{:S(2)}) async-start(bf16[8,2,20,1024]{3,1,2,0:T(2,128)(2,1)} %copy.62), calls=%async_computation.1 | async-start | bytes 1310720 | tf_op jit(solution)/shard_map/all_to_all | solution.py:76
  41.5 35.3 %reduce-scatter.11.cloned.1.call-start = ((), (), s32[]{:S(2)}) async-start(), calls=%async_computation.13 | async-start | bytes 327680 | tf_op jit(solution)/shard_map/reduce_scatter | solution.py:99
  43.8 60.7 %reduce-scatter.9.cloned.1.call-start = ((), (), s32[]{:S(2)}) async-start(), calls=%async_computation.12 | async-start | bytes 327680 | tf_op jit(solution)/shard_map/reduce_scatter | solution.py:100
  46.2 130.7 %all-reduce.3.cloned.1.call-start = ((), (), s32[]{:S(2)}) async-start(), calls=%async_computation.17 | async-start | bytes 3932160 | tf_op jit(solution)/shard_map/psum | solution.py:89
  46.2 1.8 copy-start.1
  63.2 189.5 %reduce-scatter.15.cloned.1.call-start = ((), (), s32[]{:S(2)}) async-start(), calls=%async_computation.15 | async-start | bytes 2359296 | tf_op jit(solution)/shard_map/reduce_scatter | solution.py:29
  116.4 157.3 %reduce-scatter.13.cloned.1.call-start = ((), (), s32[]{:S(2)}) async-start(), calls=%async_computation.14 | async-start | bytes 2359296 | tf_op jit(solution)/shard_map/reduce_scatter | solution.py:28
  127.8 183.5 %reduce-scatter.17.cloned.1.call-start = ((), (), s32[]{:S(2)}) async-start(), calls=%async_computation.16 | async-start | bytes 2359296 | tf_op jit(solution)/shard_map/reduce_scatter | solution.py:30
  136.1 1.8 copy-start.14
  179.6 10.2 %all-to-all-start.4 = ((f32[2,8,20]{2,0,1:T(2,128)}), f32[2,8,20]{2,0,1:T(2,128)S(1)}, u32[]{:S(2)}, u32[]{:S(2)}) async-start(f32[2,8,20]{2,0,1:T(2,128)} %copy.69), calls=%async_computation.7 | async-start | bytes 16384 | tf_op jit(solution)/shard_map/all_to_all | solution.py:125
  184.2 1.7 copy-start.2
  186.7 7.7 %copy-start.9 = (s32[128,2]{1,0:T(8,128)S(1)}, s32[128,2]{1,0:T(8,128)}, u32[]{:S(2)}) copy-start(s32[128,2]{1,0:T(8,128)} %copy-done.8) | copy-start | bytes 3076
  189.8 48.5 %all-to-all-start.3 = ((f32[2,160,1024]{2,0,1:T(2,128)}), f32[2,160,1024]{2,0,1:T(2,128)}, u32[]{:S(2)}, u32[]{:S(2)}) async-start(f32[2,160,1024]{2,0,1:T(2,128)} %copy.67), calls=%async_computation.3 | async-start | bytes 2621440 | tf_op jit(solution)/shard_map/all_to_all | solution.py:124
  197.3 12.4 %copy-start.13 = (s32[1024]{0:T(1024)}, s32[1024]{0:T(1024)S(1)}, u32[]{:S(2)}) copy-start(s32[1024]{0:T(1024)S(1)} %pad_clamp_fusion) | copy-start | bytes 12292
  202.7 2.9 copy-start.5
  202.7 2.9 copy-start.6
  244.8 5.7 %copy-start.4 = (bf16[1024,512]{1,0:T(8,128)(2,1)S(1)}, bf16[1024,512]{1,0:T(8,128)(2,1)}, u32[]{:S(2)}) copy-start(bf16[1024,512]{1,0:T(8,128)(2,1)} %param.18) | copy-start | bytes 3145732
  244.8 5.7 %copy-start.11 = (bf16[128,512]{1,0:T(8,128)(2,1)S(1)}, bf16[128,512]{1,0:T(8,128)(2,1)}, u32[]{:S(2)}) copy-start(bf16[128,512]{1,0:T(8,128)(2,1)} %copy-done.10) | copy-start | bytes 393220
  (2 other events, 1.3 us)
Sparse Core Ops, SparseCore 0:
  23.3 25.7 reduce-scatter.6
  52.4 24.3 reduce-scatter.10
  80.2 24.3 reduce-scatter.8
  108.4 68.4 all-reduce.2
  179.6 46.3 reduce-scatter.14
  228.8 44.9 reduce-scatter.12
  276.6 34.6 reduce-scatter.16
where the time goes:
time: 319 us; the launch traced here: 318 us
  waiting for transfers between devices  171 us (54%)
  matrix products  37.4 us (12%)
  blocking collectives  35.6 us (11%)
  local copies, waits for them, and re-layouts  32.1 us (10%)
  starting transfers between devices  19.9 us (6%)
  between operations  14.4 us (5%)
  other arithmetic  7.71 us (2%)
    reduce_scatter x1, waiting for transfers between devices, shared_weight_sums(): lax.psum_scatter(local_down, 'ep', scatter_dimension=0, tiled=True)  37.6 us
    psum x1, waiting for transfers between devices, body(): lax.psum((part_gate, part_up, part_down), 'tp')  28.3 us
    reduce_scatter x1, waiting for transfers between devices, body(): lax.psum_scatter(shared_part_up, 'tp', scatter_dimension=1, tiled=True)  27.7 us
    all_to_all x1, waiting for transfers between devices, body(): lax.all_to_all(slot_grad, 'ep', split_axis=1, concat_axis=0, tiled=True)  25.8 us
    reduce_scatter x1, waiting for transfers between devices, shared_weight_sums(): lax.psum_scatter(local_gate, 'ep', scatter_dimension=1, tiled=True)  21.1 us
    reduce_scatter x1, waiting for transfers between devices, body(): lax.psum_scatter(shared_part_gate, 'tp', scatter_dimension=1, tiled=True)  13.6 us
    all_to_all x1, waiting for transfers between devices, body(): lax.all_to_all(send_cotan, 'ep', split_axis=0, concat_axis=2, tiled=True)  10.3 us
    all_to_all x1, blocking collectives, body(): lax.all_to_all(send_gates, 'ep', split_axis=0, concat_axis=2, tiled=True)  9.99 us
  transfers between devices with their start and end apart: 11, of which 9 were waited for; matrix products, arithmetic and copies ran while one was open for 22% of the time, Pallas kernels for 0%

commit v1 on v0

v1 whole, which is shorter than its diff:
```python
import functools

import jax
import jax.numpy as jnp
from jax import lax
from jax.experimental import pallas as pl
from jax.experimental.pallas import tpu as pltpu
from jax.sharding import PartitionSpec as P

CORES = 2
BF = jnp.bfloat16
F32 = jnp.float32


def up_to(value, unit):
    return -(-value // unit) * unit


def dot(a, b):
    return jnp.dot(a, b, preferred_element_type=F32)


def dot_t(a, b):
    return lax.dot_general(a, b, (((1,), (1,)), ((), ())), preferred_element_type=F32)


def hidden_terms(gate_pre, up_pre, back_grad, scaling):
    logistic = jax.nn.sigmoid(gate_pre)
    silu = gate_pre * logistic
    product = silu * up_pre
    grad_act = back_grad if scaling is None else scaling * back_grad
    gate_grad = grad_act * up_pre * logistic * (1.0 + gate_pre * (1.0 - logistic))
    hidden = product if scaling is None else scaling * product
    return (
        gate_grad.astype(BF),
        (grad_act * silu).astype(BF),
        hidden.astype(BF),
        jnp.sum(back_grad * product, axis=-1, keepdims=True),
    )


def ring_plan(length):
    plan = []
    for step in range(1, length // 2 + 1):
        last_even = length % 2 == 0 and step == length // 2
        plan.append((step, 0, (0,) if last_even else (0, 1)))
        plan.append((step, 1, (1,) if last_even else (1, 0)))
    return plan


def kernel(
    dims,
    meta_in,
    home_in,
    tok_in,
    cot_in,
    eg_in,
    eu_in,
    ed_in,
    sg_in,
    su_in,
    sd_in,
    gtok_out,
    gw_out,
    osg,
    osu,
    osd,
    stok,
    scot,
    hg,
    hu,
    hh,
    all_tok,
    all_cot,
    all_meta,
    eg,
    eu,
    ed,
    sg,
    su,
    sd,
    sel,
    gates,
    sh_part,
    sh_recv,
    sh_all,
    share_t,
    part,
    recv,
    dgs,
    sgrad,
    back_send,
    back,
    shsum,
    load_sem,
    own_sem,
    ring_s,
    ring_r,
    mate_s,
    mate_r,
    shr_s,
    shr_r,
    sha_s,
    sha_r,
    pr_s,
    pr_r,
    pa_s,
    pa_r,
    xt_s,
    xt_r,
    bk_s,
    bk_r,
):
    ep, tp, tok, dl, ne, ff, sff, cap, re, rows, rpp, rpt, hp, swid = dims
    me = lax.axis_index("ep")
    mt = lax.axis_index("tp")
    length = ep // CORES
    chip = me // CORES
    core = me % CORES
    mate = chip * CORES + (1 - core)
    nxt = ((chip + 1) % length) * CORES + core
    prv = ((chip + length - 1) % length) * CORES + core

    owns = []
    for n, (src, dst) in enumerate(((tok_in, all_tok), (cot_in, all_cot), (meta_in, all_meta))):
        c = pltpu.make_async_copy(src, dst.at[me], own_sem.at[n])
        c.start()
        owns.append(c)
    loads = []
    for n, (src, dst) in enumerate(
        ((sg_in, sg), (su_in, su), (sd_in, sd), (eg_in, eg), (eu_in, eu), (ed_in, ed))
    ):
        c = pltpu.make_async_copy(src, dst, load_sem.at[n])
        c.start()
        loads.append(c)

    barrier = pltpu.get_barrier_semaphore()
    for o in range(1, ep):
        pl.semaphore_signal(barrier, inc=1, device_id={"ep": (me + o) % ep})
    for o in range(1, tp):
        pl.semaphore_signal(barrier, inc=1, device_id={"tp": (mt + o) % tp})
    pl.semaphore_wait(barrier, ep + tp - 2)

    sends = []

    def remote(src, dst, ssem, rsem, dev):
        c = pltpu.make_async_remote_copy(
            src_ref=src, dst_ref=dst, send_sem=ssem, recv_sem=rsem, device_id=dev
        )
        c.start()
        sends.append(c)
        return c

    bufs = (all_tok, all_cot, all_meta)
    ring_copies = {}
    mate_copies = []
    plan = {(step, d): items for step, d, items in ring_plan(length)}

    def ring_send(step, d, item, src):
        dest = nxt if d == 0 else prv
        subs = (0, 2) if item == 0 else (1,)
        for b in subs:
            n = ((step - 1) * 2 + d) * 3 + b
            ring_copies[step, d, b] = remote(
                bufs[b].at[src], bufs[b].at[src], ring_s.at[n], ring_r.at[n], {"ep": dest}
            )

    def mate_send(item, src):
        for b in (0, 2) if item == 0 else (1,):
            n = len(mate_copies)
            mate_copies.append(
                remote(
                    bufs[b].at[src], bufs[b].at[src], mate_s.at[n], mate_r.at[n], {"ep": mate}
                )
            )

    for c in owns:
        c.wait()
    for pos in range(2):
        for d in range(2):
            items = plan.get((1, d), ())
            if pos < len(items):
                ring_send(1, d, items[pos], me)
    mate_send(0, me)
    mate_send(1, me)

    tp_order = [(mt + o) % tp for o in range(1, tp)]
    if rpt * tp > tok:
        sh_part[:, tok:, :] = jnp.zeros((3, rpt * tp - tok, sff), BF)
    for n in range(3):
        loads[n].wait()
        if n < 2:
            val = dot(all_tok[me], (sg, su)[n][...])
        else:
            val = dot_t(all_cot[me], sd[...])
        sh_part[n, :tok, :] = val.astype(BF)
    sh_copies = []
    for o in range(1, tp):
        peer = tp_order[o - 1]
        sh_copies.append(
            remote(
                sh_part.at[:, pl.ds(pl.multiple_of(peer * rpt, 16), rpt), :],
                sh_recv.at[o],
                shr_s.at[o],
                shr_r.at[o],
                {"tp": peer},
            )
        )

    def ring_arrivals(step):
        for pos in range(2):
            for d in range(2):
                items = plan.get((step, d), ())
                if pos >= len(items):
                    continue
                item = items[pos]
                away = length - step if d == 0 else step
                src = ((chip + away) % length) * CORES + core
                for b in (0, 2) if item == 0 else (1,):
                    ring_copies[step, d, b].wait_recv()
                if item in plan.get((step + 1, d), ()):
                    ring_send(step + 1, d, item, src)
                mate_send(item, src)

    if length > 1:
        ring_arrivals(1)

    for c in sh_copies:
        c.wait_recv()
    mine_t = pl.ds(pl.multiple_of(mt * rpt, 16), rpt)
    tot = [sh_part[n, mine_t, :].astype(F32) for n in range(3)]
    for o in range(1, tp):
        for n in range(3):
            tot[n] = tot[n] + sh_recv[o, n].astype(F32)
    a, b, c3, _ = hidden_terms(tot[0], tot[1], tot[2], None)
    sh_all[0, mine_t, :] = a
    sh_all[1, mine_t, :] = b
    sh_all[2, mine_t, :] = c3
    sha = []
    for o in range(1, tp):
        sha.append(
            remote(
                sh_all.at[:, mine_t, :],
                sh_all.at[:, mine_t, :],
                sha_s.at[o],
                sha_r.at[o],
                {"tp": tp_order[o - 1]},
            )
        )

    for step in range(2, length // 2 + 1):
        ring_arrivals(step)
    for c in mate_copies:
        c.wait_recv()

    row_id = lax.broadcasted_iota(jnp.int32, (rows, tok), 0)
    gate = jnp.zeros((rows, 1), F32)
    for j in range(ep):
        m = all_meta[j]
        code = m[0:2, :].astype(jnp.int32) + (j * cap - me * (ne * re))
        p0 = (row_id == code[0:1, :]).astype(F32)
        p1 = (row_id == code[1:2, :]).astype(F32)
        sel[:, j * tok : (j + 1) * tok] = (p0 + p1).astype(BF)
        gate = gate + jnp.sum(p0 * m[2:3, :] + p1 * m[3:4, :], axis=1, keepdims=True)
    gates[:rows, :] = jnp.broadcast_to(gate, (rows, 128))
    total_rows = rpp * tp
    if total_rows > rows:
        gates[rows:, :] = jnp.zeros((total_rows - rows, 128), F32)
        part[:, rows:, :] = jnp.zeros((3, total_rows - rows, ff), BF)

    p_copies = []

    def push(n):
        for o in range(1, tp):
            peer = tp_order[o - 1]
            p_copies.append(
                remote(
                    part.at[n, pl.ds(pl.multiple_of(peer * rpp, 16), rpp), :],
                    recv.at[o, n],
                    pr_s.at[n * tp + o],
                    pr_r.at[n * tp + o],
                    {"tp": peer},
                )
            )

    stok[...] = dot(sel[...], all_tok[...].reshape(ep * tok, dl)).astype(BF)
    for n in range(2):
        loads[3 + n].wait()
        for e in range(ne):
            part[n, e * re : (e + 1) * re, :] = dot(
                stok[e * re : (e + 1) * re, :], (eg, eu)[n][e]
            ).astype(BF)
        push(n)
    scot[...] = dot(sel[...], all_cot[...].reshape(ep * tok, dl)).astype(BF)
    loads[5].wait()
    for e in range(ne):
        part[2, e * re : (e + 1) * re, :] = dot_t(scot[e * re : (e + 1) * re, :], ed[e]).astype(BF)
    push(2)

    for c in sha:
        c.wait_recv()
    for n in range(3):
        back_t = sh_all[n, :tok, :].astype(F32).T.astype(BF)
        for j in range(ep):
            share_t[0, n, j] = back_t[j * swid : (j + 1) * swid, :]
    xts = []
    for o in range(1, ep):
        peer = (me + o) % ep
        xts.append(
            remote(
                share_t.at[0, :, peer],
                share_t.at[1, :, me],
                xt_s.at[o],
                xt_r.at[o],
                {"ep": peer},
            )
        )
    for n in range(3):
        share_t[1, n, me] = share_t[0, n, me]
    shsum[...] = dot_t(sh_all[0, :tok, :], sg[...]) + dot_t(sh_all[1, :tok, :], su[...])

    for c in p_copies:
        c.wait_recv()
    mine = pl.ds(pl.multiple_of(mt * rpp, 16), rpp)
    tot = [part[n, mine, :].astype(F32) for n in range(3)]
    for o in range(1, tp):
        for n in range(3):
            tot[n] = tot[n] + recv[o, n].astype(F32)
    a, b, c3, dg = hidden_terms(tot[0], tot[1], tot[2], gates[mine, :][:, 0:1])
    hg[mine, :] = a
    hu[mine, :] = b
    hh[mine, :] = c3
    high = dg.astype(BF).astype(F32)
    lane = lax.broadcasted_iota(jnp.int32, (rpp, 128), 1)
    dgs[mine, :] = jnp.where(lane == 0, high, jnp.where(lane == 1, dg - high, 0.0)).astype(BF)
    pas = []
    for k, buf in enumerate((hg, hu, dgs, hh)):
        for o in range(1, tp):
            pas.append(
                remote(
                    buf.at[mine, :],
                    buf.at[mine, :],
                    pa_s.at[k * tp + o],
                    pa_r.at[k * tp + o],
                    {"tp": tp_order[o - 1]},
                )
            )

    for c in xts:
        c.wait_recv()
    flat = [
        jnp.concatenate([share_t[1, n, j] for j in range(ep)], axis=1) for n in range(3)
    ]
    tok_flat = all_tok[...].reshape(ep * tok, dl)
    osg[...] = dot(flat[0], tok_flat).T
    osu[...] = dot(flat[1], tok_flat).T
    osd[...] = dot(flat[2], all_cot[...].reshape(ep * tok, dl))

    for c in pas[: 3 * (tp - 1)]:
        c.wait_recv()
    for e in range(ne):
        r = slice(e * re, (e + 1) * re)
        sgrad[r, :dl] = (dot_t(hg[r, :], eg[e]) + dot_t(hu[r, :], eu[e])).astype(BF)
    sgrad[:, dl:] = dgs[:rows, :]
    col = lax.broadcasted_iota(jnp.int32, (8, rows), 1)
    expert = jnp.zeros((8, rows), jnp.int32)
    for e in range(1, ne):
        expert = expert + (col >= e * re).astype(jnp.int32)
    within = col - expert * re
    block = jnp.zeros((8, rows), jnp.int32)
    for j in range(1, ep):
        block = block + (within >= j * cap).astype(jnp.int32)
    target = block * hp + expert * cap + (within - block * cap)
    target = jnp.where(within < ep * cap, target, -1)
    pick = (
        (lax.broadcasted_iota(jnp.int32, (ep * hp, rows), 0) == target[0:1, :])
        .astype(F32)
        .astype(BF)
    )
    back_send[...] = dot(pick, sgrad[...]).astype(BF).reshape(ep, hp, dl + 128)
    bks = []
    for o in range(1, ep):
        peer = (me + o) % ep
        bks.append(
            remote(back_send.at[peer], back.at[me], bk_s.at[o], bk_r.at[o], {"ep": peer})
        )
    back[me] = back_send[me]
    home = home_in[...]
    hcol = lax.broadcasted_iota(jnp.int32, (tok, ep * hp), 1)
    g0 = (hcol == home[:, 0:1]).astype(F32)
    g1 = (hcol == home[:, 1:2]).astype(F32)
    both = (g0 + g1).astype(BF)
    for c in bks:
        c.wait_recv()
    flat_back = back[...].reshape(ep * hp, dl + 128)
    gtok_out[...] = (dot(both, flat_back[:, :dl]) + shsum[...]).astype(BF)
    w0 = jnp.sum(dot(g0.astype(BF), flat_back[:, dl:]), axis=1, keepdims=True)
    w1 = jnp.sum(dot(g1.astype(BF), flat_back[:, dl:]), axis=1, keepdims=True)
    wl = lax.broadcasted_iota(jnp.int32, (tok, 128), 1)
    gw_out[...] = jnp.where(wl == 0, w0, w1)
    for c in pas[3 * (tp - 1) :]:
        c.wait_recv()
    for c in sends:
        c.wait_send()


def body(
    tokens,
    routes,
    route_weights,
    cotangent,
    expert_gate,
    expert_up,
    expert_down,
    shared_gate,
    shared_up,
    shared_down,
):
    tok, top = routes.shape
    dl = tokens.shape[1]
    ne, _, ff = expert_gate.shape
    sff = shared_gate.shape[1]
    ep, tp = lax.axis_size("ep"), lax.axis_size("tp")
    cap = max(2, 5 * tok * top // (4 * ep * ne))
    re = up_to(ep * cap, 16)
    rows = ne * re
    rpp = up_to(-(-rows // tp), 16)
    rpt = up_to(-(-tok // tp), 16)
    hp = up_to(ne * cap, 16)
    swid = sff // ep
    length = ep // CORES
    total = rpp * tp
    dims = (ep, tp, tok, dl, ne, ff, sff, cap, re, rows, rpp, rpt, hp, swid)

    picked = routes.T.reshape(-1)
    earlier = jnp.arange(top * tok)[None, :] < jnp.arange(top * tok)[:, None]
    same = picked[:, None] == picked[None, :]
    ranked = jnp.sum((same & earlier).astype(jnp.int32), axis=1)
    code = (picked * re + ranked).reshape(top, tok)
    home = ((picked // ne) * hp + (picked % ne) * cap + ranked).reshape(top, tok)
    gate = route_weights.astype(BF).astype(F32).T
    meta = jnp.concatenate(
        [code.astype(F32), gate, jnp.zeros((8 - 2 * top, tok), F32)], axis=0
    )

    vm = pl.BlockSpec(memory_space=pltpu.VMEM)
    hbm = pl.BlockSpec(memory_space=pl.ANY)
    dma = pltpu.SemaphoreType.DMA
    n_ring = max(1, (length // 2) * 6)
    scratch = [
        pltpu.VMEM((ep, tok, dl), BF),
        pltpu.VMEM((ep, tok, dl), BF),
        pltpu.VMEM((ep, 8, tok), F32),
        pltpu.VMEM(expert_gate.shape, BF),
        pltpu.VMEM(expert_up.shape, BF),
        pltpu.VMEM(expert_down.shape, BF),
        pltpu.VMEM(shared_gate.shape, BF),
        pltpu.VMEM(shared_up.shape, BF),
        pltpu.VMEM(shared_down.shape, BF),
        pltpu.VMEM((rows, ep * tok), BF),
        pltpu.VMEM((total, 128), F32),
        pltpu.VMEM((3, rpt * tp, sff), BF),
        pltpu.VMEM((tp, 3, rpt, sff), BF),
        pltpu.VMEM((3, rpt * tp, sff), BF),
        pltpu.VMEM((2, 3, ep, swid, tok), BF),
        pltpu.VMEM((3, total, ff), BF),
        pltpu.VMEM((tp, 3, rpp, ff), BF),
        pltpu.VMEM((total, 128), BF),
        pltpu.VMEM((rows, dl + 128), BF),
        pltpu.VMEM((ep, hp, dl + 128), BF),
        pltpu.VMEM((ep, hp, dl + 128), BF),
        pltpu.VMEM((tok, dl), F32),
        dma((6,)),
        dma((3,)),
        dma((n_ring,)),
        dma((n_ring,)),
        dma((3 * length,)),
        dma((3 * length,)),
        dma((tp,)),
        dma((tp,)),
        dma((tp,)),
        dma((tp,)),
        dma((3 * tp,)),
        dma((3 * tp,)),
        dma((4 * tp,)),
        dma((4 * tp,)),
        dma((ep,)),
        dma((ep,)),
        dma((ep,)),
        dma((ep,)),
    ]
    sds = jax.ShapeDtypeStruct
    outs = pl.pallas_call(
        functools.partial(kernel, dims),
        out_shape=(
            sds((tok, dl), BF),
            sds((tok, 128), F32),
            sds((dl, swid), F32),
            sds((dl, swid), F32),
            sds((swid, dl), F32),
            sds((rows, dl), BF),
            sds((rows, dl), BF),
            sds((total, ff), BF),
            sds((total, ff), BF),
            sds((total, ff), BF),
        ),
        in_specs=[hbm, vm] + [hbm] * 8,
        out_specs=tuple([vm] * 10),
        scratch_shapes=scratch,
        compiler_params=pltpu.CompilerParams(
            collective_id=0, has_side_effects=True, vmem_limit_bytes=60 * 1024 * 1024
        ),
    )(
        meta,
        home.T,
        tokens,
        cotangent,
        expert_gate,
        expert_up,
        expert_down,
        shared_gate,
        shared_up,
        shared_down,
    )
    gtok, gw, osg, osu, osd, stok, scot, hg, hu, hh = outs
    stok = stok.reshape(ne, re, dl)
    scot = scot.reshape(ne, re, dl)
    hg, hu, hh = (h[:rows].reshape(ne, re, ff) for h in (hg, hu, hh))
    grad_gate = jnp.einsum("esd,esf->edf", stok, hg, preferred_element_type=F32)
    grad_up = jnp.einsum("esd,esf->edf", stok, hu, preferred_element_type=F32)
    grad_down = jnp.einsum("esf,esd->efd", hh, scot, preferred_element_type=F32)
    return gtok, gw[:, :top], grad_gate, grad_up, grad_down, osg, osu, osd


def solution(mesh):
    return jax.shard_map(
        body,
        mesh=mesh,
        in_specs=(
            P("ep", "tp"),
            P("ep", None),
            P("ep", None),
            P("ep", "tp"),
            P("ep", "tp", None),
            P("ep", "tp", None),
            P("ep", None, "tp"),
            P("tp", None),
            P("tp", None),
            P(None, "tp"),
        ),
        out_specs=(
            P("ep", "tp"),
            P("ep", None),
            P("ep", "tp", None),
            P("ep", "tp", None),
            P("ep", None, "tp"),
            P("tp", "ep"),
            P("tp", "ep"),
            P("ep", "tp"),
        ),
        check_vma=False,
    )
```

time: 319 us -> 115 us (0.36)
  the two profiles are of different devices: /device:TPU:0 before, /device:TPU:9 now
where the time goes in v1:
time: 115 us; the launch traced here: 114 us
  Pallas kernels  93.9 us (82%)
  matrix products  9.71 us (8%)
  local copies, waits for them, and re-layouts  7.94 us (7%)
  other arithmetic  2.28 us (2%)
    pallas_call x1, Pallas kernels, body(): pl.pallas_call(functools.partial(kernel, dims), out_shape=(sds((tok, dl),...  93.9 us
    unnamed x18, local copies, waits for them, and re-layouts  7.63 us
    dot_general x1, matrix products, body(): grad_up = jnp.einsum('esd,esf->edf', stok, hu, preferred_element_type=F32)  4.09 us
    dot_general x1, matrix products, body(): grad_gate = jnp.einsum('esd,esf->edf', stok, hg, preferred_element_type=F32)  2.84 us
    dot_general x1, matrix products, body(): grad_down = jnp.einsum('esf,esd->efd', hh, scot, preferred_element_type=F32)  2.78 us

profile of v1, /device:TPU:9, one launch (start us, length us, event | category | flops | bytes accessed | tf_op | source)
XLA Modules:
  0.0 114.5 jit_solution(3549601167908934842)
XLA Ops:
  0.6 0.1 pad.2.clone
  0.7 0.7 convert_bitcast_fusion
  1.4 0.8 copy.39
  2.2 0.1 copy.41
  2.2 0.2 convert_reduce_fusion
  2.4 0.1 copy.42
  2.6 0.7 fusion.4
  3.3 0.1 copy.43
  3.3 0.7 maximum_maximum_fusion.meta_in
  4.0 93.9 %shard_map.161 = (bf16[128,1024]{1,0:T(8,128)(2,1)}, f32[128,128]{1,0:T(8,128)}, f32[1024,64]{1,0:T(8,128)}, f32[1024,64]{1,0:T(8,128)}, f32[64,1024]{1,0:T(8,12...) custom-call(f32[8,128]{1,0:T(8,128)} %maximum_maximum_fusion.meta_in, ...), custom_call_target="tpu_custom_call" | custom-call | tf_op jit(solution)/shard_map/pallas_call | solution.py:493
  97.9 0.0 copy-start
  97.9 0.0 copy-start.3
  97.9 1.6 %copy.46 = f32[128,2]{0,1:T(2,128)} copy(f32[128,2]{1,0:T(8,128)} %bitcast.28) | data formatting | bytes 2048
  99.5 1.9 %copy.47 = f32[1024,64]{0,1:T(8,128)} copy(f32[1024,64]{1,0:T(8,128)} %get-tuple-element.57) | data formatting | bytes 524288
  101.4 1.9 %copy.48 = f32[1024,64]{0,1:T(8,128)} copy(f32[1024,64]{1,0:T(8,128)} %get-tuple-element.58) | data formatting | bytes 524288
  103.3 4.1 %fusion.11 = f32[2,1024,512]{2,1,0:T(8,128)} fusion(bf16[2,160,1024]{2,1,0:T(8,128)(2,1)} %bitcast.21, bf16[2,160,512]{2,1,0:T(8,128)(2,1)} %bitcast.27), kind=kOutput, calls=%fused_computation.22 | convolution fusion | flops 335544320 | bytes 5177344 | tf_op jit(solution)/shard_map/esd,esf->edf/dot_general | solution.py:530
  107.4 0.0 copy-done
  107.4 0.0 copy-done.3
  107.5 0.0 copy-start.4
  107.5 2.8 %fusion.10 = f32[2,1024,512]{2,1,0:T(8,128)} fusion(bf16[2,160,1024]{2,1,0:T(8,128)(2,1)S(1)} %bitcast.22, bf16[2,160,512]{2,1,0:T(8,128)(2,1)S(1)} %bitcast.26), kind=kOutput, calls=%fused_computation.21 | convolution fusion | flops 335544320 | bytes 5177344 | tf_op jit(solution)/shard_map/esd,esf->edf/dot_general | solution.py:529
  110.3 2.8 %fusion.12 = f32[2,512,1024]{2,1,0:T(8,128)} fusion(bf16[2,160,512]{2,1,0:T(8,128)(2,1)S(1)} %bitcast.25, bf16[2,160,1024]{2,1,0:T(8,128)(2,1)S(1)} %bitcast.23), kind=kOutput, calls=%fused_computation.23 | convolution fusion | flops 335544320 | bytes 5177344 | tf_op jit(solution)/shard_map/esf,esd->efd/dot_general | solution.py:531
  113.1 0.0 copy-done.5
  113.1 0.7 copy.51
  113.8 0.7 copy.52
  (7 shorter events, 0.0 us)
Async XLA Ops:
  97.9 9.5 %copy-start = (bf16[320,1024]{1,0:T(8,128)(2,1)S(1)}, bf16[320,1024]{1,0:T(8,128)(2,1)}, u32[]{:S(2)}) copy-start(bf16[320,1024]{1,0:T(8,128)(2,1)} %get-tuple-element.20) | copy-start | bytes 1966084
  97.9 9.5 %copy-start.3 = (bf16[320,512]{1,0:T(8,128)(2,1)S(1)}, bf16[320,512]{1,0:T(8,128)(2,1)}, u32[]{:S(2)}) copy-start(bf16[320,512]{1,0:T(8,128)(2,1)} %get-tuple-element.21) | copy-start | bytes 983044
  103.3 7.0 %copy-start.1 = (bf16[320,1024]{1,0:T(8,128)(2,1)S(1)}, bf16[320,1024]{1,0:T(8,128)(2,1)}, u32[]{:S(2)}) copy-start(bf16[320,1024]{1,0:T(8,128)(2,1)} %get-tuple-element.24) | copy-start | bytes 1966084
  103.3 7.0 %copy-start.2 = (bf16[320,512]{1,0:T(8,128)(2,1)S(1)}, bf16[320,512]{1,0:T(8,128)(2,1)}, u32[]{:S(2)}) copy-start(bf16[320,512]{1,0:T(8,128)(2,1)} %get-tuple-element.23) | copy-start | bytes 983044
  107.4 5.6 %copy-start.5 = (bf16[128,1024]{1,0:T(8,128)(2,1)S(1)}, bf16[128,1024]{1,0:T(8,128)(2,1)}, u32[]{:S(2)}) copy-start(bf16[128,1024]{1,0:T(8,128)(2,1)} %get-tuple-element.70) | copy-start | bytes 786436
  107.5 6.3 %copy-start.4 = (f32[64,1024]{1,0:T(8,128)S(1)}, f32[64,1024]{1,0:T(8,128)}, u32[]{:S(2)}) copy-start(f32[64,1024]{1,0:T(8,128)} %get-tuple-element.77) | copy-start | bytes 786436
